TPU v7x, 32 devices: a whole 2x2x4 slice. The times are simulated.
32 devices in a mesh: sp: 4 (over y, x), tp: 8 (over z, core).
Axes of the slice: x: 2, y: 2, z: 4, core: 2. Of those that a mesh axis runs over, the one named last changes fastest.
Arguments:
- pool_input: bfloat16 [16384, 512], P('sp', 'tp'), may hold values from -6 to 6
- gate_pre: bfloat16 [16384, 1024], P(('sp', 'tp')), may hold values from -8 to 8
- resid: bfloat16 [16384, 1024], P(('sp', 'tp')), may hold values from -6 to 6
- docs: int32 [16384], P('sp'), may hold values from 0 to 3, never falling along the last dimension, each value on 1 to 8192 neighbouring positions
- w_up: bfloat16 [512, 1024], replicated, may hold values from -0.25 to 0.25
- w_out: bfloat16 [1024, 1024], replicated, may hold values from -0.1875 to 0.1875
- g_ffn: float32 [1024], replicated, may hold values from 0.1 to 1.9
- w_gate: bfloat16 [4, 1024, 1024], P('sp'), may hold values from -0.5 to 0.5
- w_lift: bfloat16 [4, 1024, 1024], P('sp'), may hold values from -0.5 to 0.5
- w_down: bfloat16 [4, 1024, 1024], P('sp'), may hold values from -0.0390625 to 0.0390625
- routes: int32 [16384, 2], P(('sp', 'tp')), may hold values from 0 to 3, all different within a row; in each aligned block of 512 rows (0 to 511, 512 to 1023, ...) at most 320 rows name the same one
- route_weight: float32 [16384, 2], P(('sp', 'tp')), may hold values from 0.2 to 1
Outputs:
- layer_out: bfloat16 [16384, 1024], P(('sp', 'tp'))
Inputs may be any that keep to these rules, and one draw needn't show every extreme that they name: `routes`: each row names 2 different experts; among the 512 rows of one device no expert is named more than 320 times. `docs`: document numbers never fall along the sequence.
All inputs are finite; a program needn't handle non-finite values.
Results may differ from a plain program's by a relative error of at most 0.0075.
Values may be sent and summed in bfloat16 or wider, within the bound.
No kernel may reach another device: no remote copies, remote signals or barrier semaphores. Data moves between devices by JAX's collectives and lax.ppermute only.
A program may use at most 128 MiB of HBM per device.

v0:
```python
import jax
import jax.numpy as jnp
from jax import lax
from jax.sharding import PartitionSpec as P

POOL_W = 512
RIM = 15


def shifted_2(value, axis, steps):
    count = lax.axis_size(axis)
    leading, last = (max(0, -steps), min(count, count - steps))
    return lax.ppermute(value, axis, [(source, source + steps) for source in range(leading, last)])


def on_device(
    pool_input,
    gate_pre,
    resid,
    docs,
    w_up,
    w_out,
    g_ffn,
    w_gate,
    w_lift,
    w_down,
    routes,
    route_weight,
):
    tok_dev = pool_input.shape[0]
    channels = pool_input.shape[1]
    group_size = POOL_W // 4
    channel_ids = lax.axis_index("tp") * channels + lax.iota(jnp.int32, channels)
    window = jnp.power(2, channel_ids // group_size + 1)
    edge_rows = (pool_input[tok_dev - RIM :], docs[tok_dev - RIM :])
    before_rows, before_docs = shifted_2((edge_rows[0], edge_rows[1]), "sp", 1)
    first_dev = lax.axis_index("sp") == 0
    before_docs = jnp.where(first_dev, -1, before_docs)
    values = pool_input.astype(jnp.float32)
    padded = jnp.concatenate([before_rows.astype(jnp.float32), values], axis=0)
    doc_padded = jnp.concatenate([before_docs.astype(jnp.int32), docs], axis=0)
    running = jnp.zeros((tok_dev, channels), jnp.float32)
    counts = jnp.zeros((tok_dev, channels), jnp.float32)
    for offset in range(RIM + 1):
        shifted = padded[RIM - offset : RIM - offset + tok_dev]
        same_doc = (doc_padded[RIM - offset : RIM - offset + tok_dev] == docs).astype(jnp.float32)
        weight_mask = same_doc[:, None] * (offset < window).astype(jnp.float32)[None, :]
        running = running + weight_mask * shifted
        counts = counts + weight_mask
    pooled = (running / counts - values).astype(jnp.bfloat16)
    row_count = gate_pre.shape[0]
    tokens_pooled = lax.all_to_all(pooled, "tp", split_axis=0, concat_axis=1, tiled=True)
    lifted = jnp.dot(tokens_pooled, w_up, preferred_element_type=jnp.float32)
    gated_rows = (jax.nn.sigmoid(gate_pre.astype(jnp.float32)) * lifted).astype(jnp.bfloat16)
    mixed_rows = (
        resid.astype(jnp.float32) + jnp.dot(gated_rows, w_out, preferred_element_type=jnp.float32)
    ).astype(jnp.bfloat16)
    mixed_f = mixed_rows.astype(jnp.float32)
    normed = (
        mixed_f * lax.rsqrt(jnp.mean(mixed_f * mixed_f, axis=-1, keepdims=True) + 1e-06) * g_ffn
    ).astype(jnp.bfloat16)
    model_dim = normed.shape[1]
    top_count = routes.shape[1]
    local_experts = w_gate.shape[0]
    sp_count = lax.axis_size("sp")
    experts = sp_count * local_experts
    capacity = max(2, 5 * row_count * top_count // (4 * experts))
    flat_ids = routes.reshape(-1)
    onehot = (flat_ids[:, None] == lax.iota(jnp.int32, experts)[None, :]).astype(jnp.int32)
    slot_rank = jnp.sum((jnp.cumsum(onehot, axis=0) - onehot) * onehot, axis=1)
    slot_index = flat_ids * capacity + slot_rank
    source = normed[lax.iota(jnp.int32, row_count * top_count) // top_count]
    buffer = jnp.zeros((experts * capacity, model_dim), jnp.bfloat16).at[slot_index].set(source)
    buffer = buffer.reshape(sp_count, local_experts, capacity, model_dim)
    arrived = lax.all_to_all(buffer, "sp", split_axis=0, concat_axis=0, tiled=True)
    gate_act = jnp.minimum(
        jnp.einsum("sekd,edh->sekh", arrived, w_gate, preferred_element_type=jnp.float32), 7.0
    )
    lift = jnp.clip(
        jnp.einsum("sekd,edh->sekh", arrived, w_lift, preferred_element_type=jnp.float32), -7.0, 7.0
    )
    act = ((lift + 1.0) * gate_act * jax.nn.sigmoid(1.702 * gate_act)).astype(jnp.bfloat16)
    results = jnp.einsum("sekh,ehd->sekd", act, w_down, preferred_element_type=jnp.float32).astype(
        jnp.bfloat16
    )
    returned = lax.all_to_all(results, "sp", split_axis=0, concat_axis=0, tiled=True)
    picked = returned.reshape(experts * capacity, model_dim)[slot_index].astype(jnp.float32)
    picked = picked * route_weight.reshape(-1)[:, None]
    combined = jnp.sum(picked.reshape(row_count, top_count, model_dim), axis=1)
    return (mixed_f + combined).astype(jnp.bfloat16)


def solution(mesh):
    in_specs = (
        P("sp", "tp"),
        P(("sp", "tp"), None),
        P(("sp", "tp"), None),
        P("sp"),
        P(),
        P(),
        P(),
        P("sp", None, None),
        P("sp", None, None),
        P("sp", None, None),
        P(("sp", "tp"), None),
        P(("sp", "tp"), None),
    )
    out_specs = P(("sp", "tp"), None)
    return jax.shard_map(
        on_device, mesh=mesh, in_specs=in_specs, out_specs=out_specs, check_vma=False
    )
```

profile of v0, /device:TPU:0, one launch (start us, length us, event | category | flops | bytes accessed | tf_op | source)
XLA Modules:
  0.0 173.3 jit_solution(9526131367028028698)
XLA Ops:
  0.0 0.0 copy-start
  0.0 0.0 copy-start.3
  0.0 1.4 slice.102
  1.4 5.4 %collective-permute-start = (s32[15]{0:T(128)}, s32[15]{0:T(128)}, u32[]{:S(2)}, u32[]{:S(2)}) collective-permute-start(s32[15]{0:T(128)} %slice.102), channel_id=1, source_target_pairs={{0,8},{8,16},{16,24},{1,9},{9,17},{17,25},{2,10},{10,18},{18,26},{... | collective-permute-start | bytes 188 | tf_op jit(solution)/shard_map/ppermute | solution.py:13
  6.8 0.8 slice.104
  7.6 2.9 %collective-permute-start.1 = (bf16[15,64]{0,1:T(8,128)(2,1)S(1)}, bf16[15,64]{0,1:T(8,128)(2,1)S(1)}, u32[]{:S(2)}, u32[]{:S(2)}) collective-permute-start(bf16[15,64]{0,1:T(8,128)(2,1)S(1)} %slice.104), channel_id=1, source_target_pairs={{0,8},{8,16},{16,24},{1,9},{9,17},{17,25},{2,10},{10,18},{18,26},{... | collective-permute-start | bytes 5768 | tf_op jit(solution)/shard_map/ppermute | solution.py:13
  10.7 0.5 compare_convert_fusion.14
  11.2 1.1 convert_element_type.219
  12.3 0.8 copy.25
  13.2 0.7 broadcast_multiply_fusion
  13.9 0.2 eq.93
  14.0 1.1 reduce-window.6
  15.2 0.0 collective-permute-done
  15.2 0.0 copy-done.3
  15.2 0.1 fusion.105
  15.3 0.1 fusion.104
  15.5 0.0 collective-permute-done.1
  15.5 5.8 %fusion.58 = bf16[4096,64]{0,1:T(8,128)(2,1)S(1)} fusion(f32[4096,64]{0,1:T(8,128)S(1)} %convert_element_type.219, f32[15,64]{0,1:T(8,128)S(1)} %convert_element_type.222, f32[64]{0:T(128)S(1)} %get-tuple-element.22, f32[4096]{0:T(1024)S(1)} %get-tuple-element.18, f32[64]{0:T(128)S(1)} %get-tuple-element.23, f32[4096]{0:T(1024)S(1)} %get-tuple-element.19, ...), kind=kLoop, calls=%fused_computation.114 | loop fusion | flops 20709376 | bytes 1826560 | tf_op jit(solution)/shard_map/convert_element_type | solution.py:50
  21.3 0.8 copy.33
  22.1 4.9 %all-to-all-start = ((bf16[8,512,64]{1,2,0:T(8,128)(2,1)}), bf16[8,512,64]{1,2,0:T(8,128)(2,1)S(1)}, u32[]{:S(2)}, u32[]{:S(2)}) async-start(bf16[8,512,64]{1,2,0:T(8,128)(2,1)} %bitcast.68), calls=%async_computation | async-start | bytes 1048576 | tf_op jit(solution)/shard_map/all_to_all | solution.py:52
  27.0 0.2 slice_reduce_fusion
  27.2 0.2 eq.89
  27.4 0.2 reduce-window.9
  27.6 0.1 copy.24
  27.7 0.2 mul.615
  27.9 0.1 add_bitcast_fusion
  28.1 14.3 %all-to-all-done = bf16[8,512,64]{1,2,0:T(8,128)(2,1)S(1)} async-done(((bf16[8,512,64]{1,2,0:T(8,128)(2,1)}), bf16[8,512,64]{1,2,0:T(8,128)(2,1)S(1)}, u32[]{:S(2)}, u32[]{:S(2)}) %all-to-all-start) | async-done | bytes 524320 | tf_op jit(solution)/shard_map/all_to_all | solution.py:52
  42.3 0.0 copy-start.2
  42.3 0.8 copy-done.2
  43.1 0.0 copy-start.4
  43.1 4.6 %fusion.9 = (f32[512]{0:T(512)S(1)}, bf16[512,1024]{1,0:T(8,128)(2,1)S(1)}) fusion(bf16[1024,1024]{1,0:T(8,128)(2,1)} %param.17, bf16[512,1024]{1,0:T(8,128)(2,1)} %param.13, bf16[512,512]{0,1:T(8,128)(2,1)} %bitcast.72, bf16[512,1024]{1,0:T(8,128)(2,1)} %param.16, bf16[512,1024]{1,0:T(8,128)(2,1)} %param.14), kind=kOutput, calls=%fused_computation.28 | convolution fusion | flops 1616903680 | bytes 6817792 | tf_op jit(solution)/shard_map/dot_general | solution.py:56
  47.8 0.0 copy-done.4
  47.8 1.3 fusion.11
  49.1 15.9 %scatter_custom_fusion = bf16[1280,1024]{1,0:T(8,128)(2,1)} fusion(s32[1024]{0:T(1024)S(1)} %bitcast.73, bf16[512,1024]{1,0:T(8,128)(2,1)} %fusion.11, s32[1024]{0:T(1024)S(1)} %broadcast_clamp_fusion.1, bf16[]{:T(256)} %constant.106.clone.1), kind=kCustom, calls=%fused_computation.35 | custom fusion | bytes 2621952 | tf_op jit(solution)/shard_map/scatter | solution.py:73
  65.0 34.6 %all_to_all.29 = bf16[4,1,320,1024]{3,2,1,0:T(8,128)(2,1)S(1)} all-to-all(bf16[4,1,320,1024]{3,2,1,0:T(8,128)(2,1)} %bitcast.70), channel_id=1, replica_groups=mesh['sp'=4,'tp'=8] {'sp'}, dimensions={0} | all-to-all | bytes 5242880 | tf_op jit(solution)/shard_map/all_to_all | solution.py:75
  99.6 0.0 copy-start.1
  99.6 1.5 copy-done.1
  101.2 0.0 copy-done
  101.2 4.6 %fusion = f32[4,320,1024]{2,1,0:T(8,128)} fusion(bf16[4,1,320,1024]{3,2,1,0:T(8,128)(2,1)S(1)} %all_to_all.29, bf16[1,1024,1024]{2,1,0:T(8,128)(2,1)S(1)} %copy-done), kind=kOutput, calls=%fused_computation.22 | convolution fusion | flops 2684354560 | bytes 9961472 | tf_op jit(solution)/shard_map/sekd,edh->sekh/dot_general | solution.py:77
  105.7 10.5 %convert_bitcast_fusion = bf16[4,1,320,1024]{3,2,1,0:T(8,128)(2,1)} fusion(bf16[1,1024,1024]{2,1,0:T(8,128)(2,1)} %param.21, f32[4,320,1024]{2,1,0:T(8,128)} %fusion, bf16[4,1,320,1024]{3,2,1,0:T(8,128)(2,1)} %copy-done.1, bf16[1,1024,1024]{2,1,0:T(8,128)(2,1)} %param.20), kind=kOutput, calls=%fused_computation.26 | convolution fusion | flops 5383127040 | bytes 14680064 | tf_op jit(solution)/shard_map/sekh,ehd->sekd/dot_general | solution.py:83
  116.3 0.0 copy-start.5
  116.3 4.7 %all-to-all-start.2 = ((bf16[4,1,320,1024]{3,2,1,0:T(8,128)(2,1)}), bf16[4,1,320,1024]{3,2,1,0:T(8,128)(2,1)}, u32[]{:S(2)}, u32[]{:S(2)}) async-start(bf16[4,1,320,1024]{3,2,1,0:T(8,128)(2,1)} %convert_bitcast_fusion), calls=%async_computation.2 | async-start | bytes 5242880 | tf_op jit(solution)/shard_map/all_to_all | solution.py:86
  120.9 0.0 copy-done.5
  120.9 0.1 copy.28
  121.1 29.8 %all-to-all-done.2 = bf16[4,1,320,1024]{3,2,1,0:T(8,128)(2,1)} async-done(((bf16[4,1,320,1024]{3,2,1,0:T(8,128)(2,1)}), bf16[4,1,320,1024]{3,2,1,0:T(8,128)(2,1)}, u32[]{:S(2)}, u32[]{:S(2)}) %all-to-all-start.2) | async-done | bytes 2621472 | tf_op jit(solution)/shard_map/all_to_all | solution.py:86
  150.9 8.1 %gather_fusion = bf16[1024,1024]{1,0:T(8,128)(2,1)} fusion(bf16[1280,1024]{1,0:T(8,128)(2,1)} %bitcast.18, s32[1024]{0:T(1024)S(1)} %broadcast_clamp_fusion), kind=kCustom, calls=%fused_computation.1 | custom fusion | bytes 4198400 | tf_op jit(solution)/shard_map/gather | solution.py:87
  159.0 5.5 %reshape.280 = f32[512,2,1024]{2,1,0:T(2,128)} reshape(bf16[1024,1024]{1,0:T(8,128)(2,1)} %gather_fusion) | data formatting | bytes 6291456 | tf_op jit(solution)/shard_map/convert_element_type | solution.py:87
  164.5 7.5 %multiply_reduce_fusion = f32[512,1024]{1,0:T(8,128)S(1)} fusion(f32[512,2,1024]{2,1,0:T(2,128)} %reshape.280, f32[512,2]{1,0:T(8,128)S(1)} %copy.28), kind=kLoop, calls=%fused_computation.18 | loop fusion | flops 1572864 | bytes 6295552 | tf_op jit(solution)/shard_map/reduce_sum | solution.py:89
  172.0 1.4 fusion.12
  (16 shorter events, 0.2 us)
Async XLA Ops:
  0.0 101.2 %copy-start = (bf16[1,1024,1024]{2,1,0:T(8,128)(2,1)S(1)}, bf16[1,1024,1024]{2,1,0:T(8,128)(2,1)}, u32[]{:S(2)}) copy-start(bf16[1,1024,1024]{2,1,0:T(8,128)(2,1)} %param.19) | copy-start | bytes 6291460
  0.0 15.2 %copy-start.3 = (s32[4096]{0:T(1024)S(1)}, s32[4096]{0:T(1024)}, u32[]{:S(2)}) copy-start(s32[4096]{0:T(1024)} %param.15) | copy-start | bytes 49156
  1.4 13.8 %collective-permute-start = (s32[15]{0:T(128)}, s32[15]{0:T(128)}, u32[]{:S(2)}, u32[]{:S(2)}) collective-permute-start(s32[15]{0:T(128)} %slice.102), channel_id=1, source_target_pairs={{0,8},{8,16},{16,24},{1,9},{9,17},{17,25},{2,10},{10,18},{18,26},{... | collective-permute-start | bytes 188 | tf_op jit(solution)/shard_map/ppermute | solution.py:13
  7.6 7.8 %collective-permute-start.1 = (bf16[15,64]{0,1:T(8,128)(2,1)S(1)}, bf16[15,64]{0,1:T(8,128)(2,1)S(1)}, u32[]{:S(2)}, u32[]{:S(2)}) collective-permute-start(bf16[15,64]{0,1:T(8,128)(2,1)S(1)} %slice.104), channel_id=1, source_target_pairs={{0,8},{8,16},{16,24},{1,9},{9,17},{17,25},{2,10},{10,18},{18,26},{... | collective-permute-start | bytes 5768 | tf_op jit(solution)/shard_map/ppermute | solution.py:13
  22.1 20.2 %all-to-all-start = ((bf16[8,512,64]{1,2,0:T(8,128)(2,1)}), bf16[8,512,64]{1,2,0:T(8,128)(2,1)S(1)}, u32[]{:S(2)}, u32[]{:S(2)}) async-start(bf16[8,512,64]{1,2,0:T(8,128)(2,1)} %bitcast.68), calls=%async_computation | async-start | bytes 1048576 | tf_op jit(solution)/shard_map/all_to_all | solution.py:52
  42.3 0.8 copy-start.2
  43.1 4.6 %copy-start.4 = (f32[1024]{0:T(1024)S(1)}, f32[1024]{0:T(1024)}, u32[]{:S(2)}) copy-start(f32[1024]{0:T(1024)} %param.18) | copy-start | bytes 12292
  99.6 1.5 copy-start.1
  116.3 4.7 %copy-start.5 = (f32[512,2]{0,1:T(2,128)S(1)}, f32[512,2]{0,1:T(2,128)}, u32[]{:S(2)}) copy-start(f32[512,2]{0,1:T(2,128)} %param.23) | copy-start | bytes 12292
  116.3 34.6 %all-to-all-start.2 = ((bf16[4,1,320,1024]{3,2,1,0:T(8,128)(2,1)}), bf16[4,1,320,1024]{3,2,1,0:T(8,128)(2,1)}, u32[]{:S(2)}, u32[]{:S(2)}) async-start(bf16[4,1,320,1024]{3,2,1,0:T(8,128)(2,1)} %convert_bitcast_fusion), calls=%async_computation.2 | async-start | bytes 5242880 | tf_op jit(solution)/shard_map/all_to_all | solution.py:86
where the time goes:
time: 174 us; the launch traced here: 173 us
  waiting for transfers between devices  44.1 us (25%)
  local copies, waits for them, and re-layouts  36.7 us (21%)
  blocking collectives  34.6 us (20%)
  other arithmetic  20.2 us (12%)
  matrix products  19.7 us (11%)
  starting transfers between devices  17.8 us (10%)
    all_to_all x1, blocking collectives, on_device(): lax.all_to_all(buffer, 'sp', split_axis=0, concat_axis=0, tiled=True)  34.6 us
    all_to_all x1, waiting for transfers between devices, on_device(): lax.all_to_all(results, 'sp', split_axis=0, concat_axis=0, tiled=True)  29.8 us
    scatter x1, local copies, waits for them, and re-layouts, on_device(): jnp.zeros((experts * capacity, model_dim), jnp.bfloat16).at[slot_index]  15.9 us
    all_to_all x1, waiting for transfers between devices, on_device(): lax.all_to_all(pooled, 'tp', split_axis=0, concat_axis=1, tiled=True)  14.3 us
    dot_general x1, matrix products, on_device(): jnp.einsum('sekh,ehd->sekd', act, w_down, preferred_element_type=jnp.floa...  10.5 us
    ppermute x2, starting transfers between devices, shifted_2(): lax.ppermute(value, axis, [(source, source + steps) for source in range(l...  8.26 us
    gather x1, local copies, waits for them, and re-layouts, on_device(): returned.reshape(experts * capacity, model_dim)[slot_index]  8.12 us
    reduce_sum x1, other arithmetic, on_device(): combined = jnp.sum(picked.reshape(row_count, top_count, model_dim), axis=1)  7.51 us
  transfers between devices with their start and end apart: 4, of which 2 were waited for; matrix products, arithmetic and copies ran while one was open for 4% of the time, Pallas kernels for 0%

commit v1 on v0

v1 whole, which is shorter than its diff:
```python
import functools

import jax
import jax.numpy as jnp
from jax import lax
from jax.experimental import pallas as pl
from jax.experimental.pallas import tpu as pltpu
from jax.sharding import PartitionSpec as P

HALO = 16
LANES = 128
CHUNKS = 2
F32 = jnp.float32
BF16 = jnp.bfloat16
VMEM = pl.BlockSpec(memory_space=pltpu.VMEM)


def params(mib):
    return pltpu.CompilerParams(vmem_limit_bytes=mib * 1024 * 1024)


def dot(a, b):
    return jnp.dot(a, b, preferred_element_type=F32)


def mixer_kernel(
    x_ref, halo_ref, docs_ref, slot_ref, gate_ref, resid_ref, up_ref, out_ref, gain_ref,
    mixed_ref, packed_ref, pooled_ref, normed_ref,
):
    sources, per, rows = x_ref.shape
    wide = rows + LANES
    group = sources * per // 4
    each = group // per
    ids = docs_ref[...]
    same = [ids == pltpu.roll(ids, 1 << level, 1) for level in range(4)]
    keep = [s.astype(F32) for s in same]
    count = jnp.ones((1, wide), F32)
    for g in range(4):
        count = count + keep[g] * pltpu.roll(count, 1 << g, 1)
        scale = 1.0 / count[:, LANES:]
        own = x_ref[g * each : (g + 1) * each].astype(F32).reshape(group, rows)
        edge = jnp.concatenate(
            [halo_ref[g * each + i].astype(F32) for i in range(each)], axis=1
        )
        edge = jnp.concatenate([jnp.zeros((LANES - HALO, group), F32), edge], axis=0)
        run = jnp.concatenate([edge.T, own], axis=1)
        for level in range(g + 1):
            run = run + keep[level] * pltpu.roll(run, 1 << level, 1)
        pooled = run[:, LANES:] * scale - own
        pooled_ref[:, g * group : (g + 1) * group] = pooled.T.astype(BF16)
    step = min(256, rows)
    for r in range(0, rows, step):
        part = slice(r, r + step)
        lifted = dot(pooled_ref[part], up_ref[...])
        gated = (jax.nn.sigmoid(gate_ref[part].astype(F32)) * lifted).astype(BF16)
        mixed = (resid_ref[part].astype(F32) + dot(gated, out_ref[...])).astype(BF16)
        mixed_ref[part] = mixed
        wide_mixed = mixed.astype(F32)
        norm = lax.rsqrt(jnp.mean(wide_mixed * wide_mixed, axis=-1, keepdims=True) + 1e-06)
        normed_ref[part] = (wide_mixed * norm * gain_ref[...]).astype(BF16)
    blocks, size, _ = packed_ref.shape
    for b in range(blocks):
        places = b * size + lax.broadcasted_iota(jnp.int32, (size, rows), 0)
        hit = jnp.zeros((size, rows), F32)
        for k in range(slot_ref.shape[0]):
            hit = jnp.where(places == slot_ref[k : k + 1, :], 1.0, hit)
        packed_ref[b] = dot(hit.astype(BF16), normed_ref[...]).astype(BF16)


def mixer(x, halo, docs, slots, gate_pre, resid, w_up, w_out, gain, blocks, size):
    rows, dim = resid.shape
    return pl.pallas_call(
        mixer_kernel,
        out_shape=(
            jax.ShapeDtypeStruct((rows, dim), BF16),
            jax.ShapeDtypeStruct((blocks, size, dim), BF16),
        ),
        in_specs=[VMEM] * 9,
        out_specs=(VMEM, VMEM),
        scratch_shapes=[
            pltpu.VMEM((rows, x.shape[0] * x.shape[1]), BF16),
            pltpu.VMEM((rows, dim), BF16),
        ],
        compiler_params=params(48),
        name="mixer",
    )(x, halo, docs, slots, gate_pre, resid, w_up, w_out, gain)


def expert_kernel(count, *refs):
    parts, (gate_ref, lift_ref, down_ref), outs = (
        refs[:count],
        refs[count : count + 3],
        refs[count + 3 : 2 * count + 3],
    )
    act_ref = refs[-1]
    rows = jnp.concatenate([p[...] for p in parts], axis=0) if count > 1 else parts[0][...]
    hidden = gate_ref.shape[1]
    step = min(256, hidden)
    for h in range(0, hidden, step):
        part = slice(h, h + step)
        gate = jnp.minimum(dot(rows, gate_ref[:, part]), 7.0)
        lift = jnp.clip(dot(rows, lift_ref[:, part]), -7.0, 7.0)
        act_ref[:, part] = ((lift + 1.0) * gate * jax.nn.sigmoid(1.702 * gate)).astype(BF16)
    size = parts[0].shape[0]
    for h in range(0, down_ref.shape[1], step):
        part = slice(h, h + step)
        done = dot(act_ref[...], down_ref[:, part]).astype(BF16)
        for i, out in enumerate(outs):
            out[:, part] = done[i * size : (i + 1) * size]


def expert(parts, w_gate, w_lift, w_down):
    count, (size, dim) = len(parts), parts[0].shape
    out = jax.ShapeDtypeStruct((size, w_down.shape[1]), BF16)
    return pl.pallas_call(
        functools.partial(expert_kernel, count),
        out_shape=(out,) * count,
        in_specs=[VMEM] * (count + 3),
        out_specs=(VMEM,) * count,
        scratch_shapes=[pltpu.VMEM((count * size, w_gate.shape[1]), BF16)],
        compiler_params=params(32),
        name="expert",
    )(*parts, w_gate, w_lift, w_down)


def combine_kernel(starts, slot_ref, weight_ref, mixed_ref, *refs):
    parts, out_ref = refs[:-1], refs[-1]
    rows, dim = mixed_ref.shape
    step = min(256, rows)
    for r in range(0, rows, step):
        span = slice(r, r + step)
        total = mixed_ref[span].astype(F32)
        for start, part in zip(starts, parts):
            size = part.shape[0]
            places = start + lax.broadcasted_iota(jnp.int32, (step, size), 1)
            hit = jnp.zeros((step, size), F32)
            for k in range(slot_ref.shape[1]):
                hit = jnp.where(
                    places == slot_ref[span, k : k + 1], weight_ref[span, k : k + 1], hit
                )
            total = total + dot(hit.astype(BF16), part[...])
        out_ref[span] = total.astype(BF16)


def combine(starts, slots, weights, mixed, parts):
    return pl.pallas_call(
        functools.partial(combine_kernel, tuple(starts)),
        out_shape=jax.ShapeDtypeStruct(mixed.shape, BF16),
        in_specs=[VMEM] * (3 + len(parts)),
        out_specs=VMEM,
        compiler_params=params(32),
        name="combine",
    )(slots, weights, mixed, *parts)


def on_device(
    pool_input,
    gate_pre,
    resid,
    docs,
    w_up,
    w_out,
    g_ffn,
    w_gate,
    w_lift,
    w_down,
    routes,
    route_weight,
):
    tok_dev, channels = pool_input.shape
    rows, dim = resid.shape
    tp_count, sp_count = lax.axis_size("tp"), lax.axis_size("sp")
    sp_at, tp_at = lax.axis_index("sp"), lax.axis_index("tp")
    top = routes.shape[1]
    experts = sp_count * w_gate.shape[0]
    cap = max(2, 5 * rows * top // (4 * experts))

    by_channel = pool_input.T.reshape(channels, tp_count, rows).transpose(1, 0, 2)
    x = lax.all_to_all(by_channel, "tp", split_axis=0, concat_axis=0, tiled=True)

    tails = pool_input.reshape(tp_count, rows, channels)[:, rows - HALO :]
    tail_docs = jnp.pad(docs[tok_dev - HALO :].astype(BF16), (0, channels - HALO))
    edge = lax.ppermute(
        jnp.concatenate([tails[-1], tail_docs[None]], axis=0),
        "sp",
        [(i, i + 1) for i in range(sp_count - 1)],
    )
    halo_out = jnp.concatenate([edge[None, :HALO], tails[:-1]], axis=0)
    halo = lax.all_to_all(halo_out, "tp", split_axis=0, concat_axis=0, tiled=True)
    before = jnp.where(sp_at == 0, -1, edge[HALO, :HALO].astype(jnp.int32))
    all_docs = jnp.concatenate([jnp.full((LANES - HALO,), -2, jnp.int32), before, docs])
    near_docs = lax.dynamic_slice(all_docs, (tp_at * rows,), (LANES + rows,))[None]

    picks = routes.T
    ids = lax.iota(jnp.int32, experts)
    named = picks[:, None, :] == ids[None, :, None]
    earlier = (lax.iota(jnp.int32, rows)[:, None] < lax.iota(jnp.int32, rows)[None, :]).astype(BF16)
    rank = dot(jnp.any(named, axis=0).astype(BF16), earlier).astype(jnp.int32)
    home = ((ids ^ sp_at) * cap)[:, None]
    slots = jnp.sum(jnp.where(named, (rank + home)[None], 0), axis=1)

    mixed, packed = mixer(
        x, halo, near_docs, slots, gate_pre, resid, w_up, w_out, g_ffn[None], sp_count, cap
    )

    weights = (w_gate[0], w_lift[0], w_down[0])
    chunks = CHUNKS if cap % (16 * CHUNKS) == 0 else 1
    size = cap // chunks

    def swap(value, offset):
        return lax.ppermute(value, "sp", [(i, i ^ offset) for i in range(sp_count)])

    starts, parts = [0], list(expert([packed[0]], *weights))
    for c in range(chunks):
        arrived = [
            swap(packed[o, c * size : (c + 1) * size], o) for o in range(1, sp_count)
        ]
        done = expert(arrived, *weights)
        parts += [swap(d, o) for d, o in zip(done, range(1, sp_count))]
        starts += [o * cap + c * size for o in range(1, sp_count)]
    return combine(starts, slots.T, route_weight, mixed, parts)


def solution(mesh):
    in_specs = (
        P("sp", "tp"),
        P(("sp", "tp"), None),
        P(("sp", "tp"), None),
        P("sp"),
        P(),
        P(),
        P(),
        P("sp", None, None),
        P("sp", None, None),
        P("sp", None, None),
        P(("sp", "tp"), None),
        P(("sp", "tp"), None),
    )
    out_specs = P(("sp", "tp"), None)
    return jax.shard_map(
        on_device, mesh=mesh, in_specs=in_specs, out_specs=out_specs, check_vma=False
    )
```

time: 174 us -> 117 us (0.67)
  blocking collectives: 34.6 us -> 0 us
  Pallas kernels: 0 us -> 23.1 us
  local copies, waits for them, and re-layouts: 36.7 us -> 13.7 us
  matrix products: 19.7 us -> 0.18 us
  other arithmetic: 20.2 us -> 0.85 us
  starting transfers between devices: 17.8 us -> 30.6 us
  waiting for transfers between devices: 44.1 us -> 48.2 us
    all_to_all x1 -> x0, blocking collectives: 34.6 us -> none  [on_device(): lax.all_to_all(buffer, 'sp', split_axis=0, concat_axis=0, tiled=True)]
    ppermute x2 -> x13, waiting for transfers between devices: 0.01 us -> 28.7 us  [the longest x12 27.4 us: swap(): return lax.ppermute(value, 'sp', [(i, i ^ offset) for i in range(sp_count)])]
    all_to_all x2, waiting for transfers between devices: 44.1 us -> 19.5 us  [the longest x1 14.7 us: on_device(): lax.all_to_all(by_channel, 'tp', split_axis=0, concat_axis=0, tiled=True)]
    pallas_call x0 -> x5, Pallas kernels: none -> 23.1 us  [the longest x3 10.5 us: expert(): pl.pallas_call(functools.partial(expert_kernel, count), out_shape=(out,)...]
    dot_general x3 -> x1, matrix products: 19.7 us -> 0.18 us  [dot(): return jnp.dot(a, b, preferred_element_type=F32)]
    scatter x1 -> x0, local copies, waits for them, and re-layouts: 15.9 us -> none  [on_device(): jnp.zeros((experts * capacity, model_dim), jnp.bfloat16).at[slot_index]]
    ppermute x2 -> x13, starting transfers between devices: 8.26 us -> 22.2 us  [the longest x12 17.3 us: swap(): return lax.ppermute(value, 'sp', [(i, i ^ offset) for i in range(sp_count)])]
    convert_element_type x16 -> x0, other arithmetic: 10.5 us -> none  [the longest x1 5.81 us: on_device(): pooled = (running / counts - values).astype(jnp.bfloat16)]
  transfers between devices with their start and end apart: 4 -> 15, of which waited for: 2 -> 11; matrix products, arithmetic and copies ran while one was open for 4% -> 3% of each run, Pallas kernels for 0% -> 9%
where the time goes in v1:
time: 117 us
  waiting for transfers between devices  48.2 us (41%)
  starting transfers between devices  30.6 us (26%)
  Pallas kernels  23.1 us (20%)
  local copies, waits for them, and re-layouts  13.7 us (12%)
    ppermute x12, waiting for transfers between devices, swap(): return lax.ppermute(value, 'sp', [(i, i ^ offset) for i in range(sp_count)])  27.4 us
    ppermute x12, starting transfers between devices, swap(): return lax.ppermute(value, 'sp', [(i, i ^ offset) for i in range(sp_count)])  17.3 us
    all_to_all x1, waiting for transfers between devices, on_device(): lax.all_to_all(by_channel, 'tp', split_axis=0, concat_axis=0, tiled=True)  14.7 us
    pallas_call x3, Pallas kernels, expert(): pl.pallas_call(functools.partial(expert_kernel, count), out_shape=(out,)...  10.5 us
    unnamed x36, local copies, waits for them, and re-layouts  9.65 us
    pallas_call x1, Pallas kernels, mixer(): pl.pallas_call(mixer_kernel, out_shape=(jax.ShapeDtypeStruct((rows, dim),...  7.79 us
    ppermute x1, starting transfers between devices, on_device(): lax.ppermute(jnp.concatenate([tails[-1], tail_docs[None]], axis=0), 'sp',...  4.88 us
    all_to_all x1, starting transfers between devices, on_device(): lax.all_to_all(halo_out, 'tp', split_axis=0, concat_axis=0, tiled=True)  4.88 us
  transfers between devices with their start and end apart: 15, of which 11 were waited for; matrix products, arithmetic and copies ran while one was open for 3% of the time, Pallas kernels for 9%

profile of v1, /device:TPU:0, one launch (start us, length us, event | category | flops | bytes accessed | tf_op | source)
XLA Modules:
  0.0 116.8 jit_solution(10255681606831174388)
XLA Ops:
  0.0 1.6 %copy.22 = bf16[4096,64]{1,0:T(8,128)(2,1)S(1)} copy(bf16[4096,64]{0,1:T(8,128)(2,1)} %param.12) | data formatting | bytes 1048576 | tf_op args[0]
  1.7 0.8 slice_convert_fusion.1
  2.4 4.9 %collective-permute-start = (bf16[17,64]{1,0:T(8,128)(2,1)S(1)}, bf16[17,64]{1,0:T(8,128)(2,1)S(1)}, u32[]{:S(2)}, u32[]{:S(2)}) collective-permute-start(bf16[17,64]{1,0:T(8,128)(2,1)S(1)} %pad_maximum_fusion.1), channel_id=1, source_target_pairs={{0,8},{8,16},{16,24},{1,9},{9,17},{17,25},{2,10},{10,18},{18,26},{... | collective-permute-start | bytes 6536 | tf_op jit(solution)/shard_map/ppermute | solution.py:183
  7.3 1.3 %collective-permute-done = bf16[17,64]{1,0:T(8,128)(2,1)S(1)} collective-permute-done((bf16[17,64]{1,0:T(8,128)(2,1)S(1)}, bf16[17,64]{1,0:T(8,128)(2,1)S(1)}, u32[]{:S(2)}, u32[]{:S(2)}) %collective-permute-start) | collective-permute-done | bytes 2208 | tf_op jit(solution)/shard_map/ppermute | solution.py:183
  8.7 0.7 reshape.19
  9.4 4.9 %all-to-all-start.1 = ((bf16[8,2,512]{2,1,0:T(2,128)(2,1)}), bf16[8,2,512]{2,1,0:T(2,128)(2,1)S(1)}, u32[]{:S(2)}, u32[]{:S(2)}) async-start(bf16[8,2,512]{2,1,0:T(2,128)(2,1)} %reshape.19), calls=%async_computation.1 | async-start | bytes 32768 | tf_op jit(solution)/shard_map/all_to_all | solution.py:189
  14.3 0.0 copy-done.12
  14.3 0.8 copy.26
  15.1 4.8 %all-to-all-done.1 = bf16[8,2,512]{2,1,0:T(2,128)(2,1)S(1)} async-done(((bf16[8,2,512]{2,1,0:T(2,128)(2,1)}), bf16[8,2,512]{2,1,0:T(2,128)(2,1)S(1)}, u32[]{:S(2)}, u32[]{:S(2)}) %all-to-all-start.1) | async-done | bytes 16416 | tf_op jit(solution)/shard_map/all_to_all | solution.py:189
  19.9 3.5 %all-to-all-start = ((bf16[8,64,512]{2,1,0:T(8,128)(2,1)}), bf16[8,64,512]{2,1,0:T(8,128)(2,1)S(1)}, u32[]{:S(2)}, u32[]{:S(2)}) async-start(bf16[8,64,512]{2,1,0:T(8,128)(2,1)} %bitcast.37), calls=%async_computation | async-start | bytes 1048576 | tf_op jit(solution)/shard_map/all_to_all | solution.py:179
  23.4 0.0 copy-done.14
  23.5 0.2 fusion
  23.7 0.0 copy-done.13
  23.7 0.1 concatenate.11
  23.8 0.1 dynamic_slice.3
  23.9 0.1 reshape.20.halo_ref
  24.0 14.7 %all-to-all-done.x_ref = bf16[8,64,512]{2,1,0:T(8,128)(2,1)S(1)} async-done(((bf16[8,64,512]{2,1,0:T(8,128)(2,1)}), bf16[8,64,512]{2,1,0:T(8,128)(2,1)S(1)}, u32[]{:S(2)}, u32[]{:S(2)}) %all-to-all-start) | async-done | bytes 524320 | tf_op jit(solution)/shard_map/all_to_all | solution.py:179
  38.7 0.0 copy-done.11
  38.7 0.0 copy-done.6
  38.7 1.2 %copy-done.7 = bf16[512,1024]{1,0:T(8,128)(2,1)S(1)} copy-done((bf16[512,1024]{1,0:T(8,128)(2,1)S(1)}, bf16[512,1024]{1,0:T(8,128)(2,1)}, u32[]{:S(2)}) %copy-start.7) | copy-done | bytes 1048600
  39.9 1.2 %copy-done.8 = bf16[512,1024]{1,0:T(8,128)(2,1)S(1)} copy-done((bf16[512,1024]{1,0:T(8,128)(2,1)S(1)}, bf16[512,1024]{1,0:T(8,128)(2,1)}, u32[]{:S(2)}) %copy-start.8) | copy-done | bytes 1048600
  41.1 7.8 %mixer.1 = (bf16[512,1024]{1,0:T(8,128)(2,1)S(1)}, bf16[4,320,1024]{2,1,0:T(8,128)(2,1)}) custom-call(bf16[8,64,512]{2,1,0:T(8,128)(2,1)S(1)} %all-to-all-done.x_ref, bf16[8,16,64]{2,1,0:T(8,128)(2,1)S(1)} %reshape.20.halo_ref, s32[1,640]{1,0:T(1,128)S(1)} %broadcast_in_dim.43.docs_ref, s32[2,512]{1,0:T(2,128)S(1)} %select_reduce_fusion.slot_ref, ...), custom_call_target="tpu_custom_call" | custom-call | tf_op jit(solution)/shard_map/mixer/pallas_call | solution.py:72
  48.9 1.8 %slice_bitcast_fusion.1 = (bf16[160,1024]{1,0:T(8,128)(2,1)S(1)}, bf16[160,1024]{1,0:T(8,128)(2,1)S(1)}, bf16[160,1024]{1,0:T(8,128)(2,1)S(1)}, bf16[160,1024]{1...) fusion(bf16[4,320,1024]{2,1,0:T(8,128)(2,1)} %get-tuple-element.14), kind=kLoop, calls=%fused_computation.5 | loop fusion | bytes 3932160 | tf_op jit(solution)/shard_map/squeeze | solution.py:216
  50.7 2.3 %collective-permute-start.7 = (bf16[160,1024]{1,0:T(8,128)(2,1)S(1)}, bf16[160,1024]{1,0:T(8,128)(2,1)S(1)}, u32[]{:S(2)}, u32[]{:S(2)}) collective-permute-start(bf16[160,1024]{1,0:T(8,128)(2,1)S(1)} %get-tuple-element.23), channel_id=1, source_target_pairs={{0,8},{8,0},{16,24},{24,16},{1,9},{9,1},{17,25},{25,17},{2,10},{10... | collective-permute-start | bytes 983048 | tf_op jit(solution)/shard_map/ppermute | solution.py:211
  53.1 1.5 %collective-permute-start.8 = (bf16[160,1024]{1,0:T(8,128)(2,1)S(1)}, bf16[160,1024]{1,0:T(8,128)(2,1)S(1)}, u32[]{:S(2)}, u32[]{:S(2)}) collective-permute-start(bf16[160,1024]{1,0:T(8,128)(2,1)S(1)} %get-tuple-element.22), channel_id=1, source_target_pairs={{0,16},{8,24},{16,0},{24,8},{1,17},{9,25},{17,1},{25,9},{2,18},{10... | collective-permute-start | bytes 983048 | tf_op jit(solution)/shard_map/ppermute | solution.py:211
  54.6 0.9 collective-permute-start.9
  55.5 1.1 collective-permute-start.1
  56.6 1.5 %collective-permute-start.2 = (bf16[160,1024]{1,0:T(8,128)(2,1)S(1)}, bf16[160,1024]{1,0:T(8,128)(2,1)S(1)}, u32[]{:S(2)}, u32[]{:S(2)}) collective-permute-start(bf16[160,1024]{1,0:T(8,128)(2,1)S(1)} %get-tuple-element.25), channel_id=1, source_target_pairs={{0,16},{8,24},{16,0},{24,8},{1,17},{9,25},{17,1},{25,9},{2,18},{10... | collective-permute-start | bytes 983048 | tf_op jit(solution)/shard_map/ppermute | solution.py:211
  58.1 3.5 %collective-permute-done.7.refs_0_ = bf16[160,1024]{1,0:T(8,128)(2,1)S(1)} collective-permute-done((bf16[160,1024]{1,0:T(8,128)(2,1)S(1)}, bf16[160,1024]{1,0:T(8,128)(2,1)S(1)}, u32[]{:S(2)}, u32[]{:S(2)}) %collective-permute-start.7) | collective-permute-done | bytes 327712 | tf_op jit(solution)/shard_map/ppermute | solution.py:211
  61.6 3.0 %collective-permute-start.3 = (bf16[160,1024]{1,0:T(8,128)(2,1)S(1)}, bf16[160,1024]{1,0:T(8,128)(2,1)S(1)}, u32[]{:S(2)}, u32[]{:S(2)}) collective-permute-start(bf16[160,1024]{1,0:T(8,128)(2,1)S(1)} %get-tuple-element.24), channel_id=1, source_target_pairs={{0,24},{8,16},{16,8},{24,0},{1,25},{9,17},{17,9},{25,1},{2,26},{10... | collective-permute-start | bytes 983048 | tf_op jit(solution)/shard_map/ppermute | solution.py:211
  64.6 5.6 %collective-permute-done.8.refs_1_ = bf16[160,1024]{1,0:T(8,128)(2,1)S(1)} collective-permute-done((bf16[160,1024]{1,0:T(8,128)(2,1)S(1)}, bf16[160,1024]{1,0:T(8,128)(2,1)S(1)}, u32[]{:S(2)}, u32[]{:S(2)}) %collective-permute-start.8) | collective-permute-done | bytes 327712 | tf_op jit(solution)/shard_map/ppermute | solution.py:211
  70.3 0.8 collective-permute-done.9.refs_2_
  71.1 0.0 copy-done.1
  71.1 0.0 copy-done.3
  71.1 0.0 copy-done
  71.1 4.1 %expert.5 = (bf16[160,1024]{1,0:T(8,128)(2,1)S(1)}, bf16[160,1024]{1,0:T(8,128)(2,1)}, bf16[160,1024]{1,0:T(8,128)(2,1)}) custom-call(bf16[160,1024]{1,0:T(8,128)(2,1)S(1)} %collective-permute-done.7.refs_0_, bf16[160,1024]{1,0:T(8,128)(2,1)S(1)} %collective-permute-done.8.refs_1_, bf16[160,1024]{1,0:T(8,128)(2,1)S(1)} %collective-permute-done.9.refs_2_, ...), custom_call_target="tpu_custom_call" | custom-call | tf_op jit(solution)/shard_map/expert/pallas_call | solution.py:115
  75.2 0.6 collective-permute-start.10
  75.8 2.0 %collective-permute-start.11 = (bf16[160,1024]{1,0:T(8,128)(2,1)}, bf16[160,1024]{1,0:T(8,128)(2,1)}, u32[]{:S(2)}, u32[]{:S(2)}) collective-permute-start(bf16[160,1024]{1,0:T(8,128)(2,1)} %get-tuple-element.19), channel_id=1, source_target_pairs={{0,16},{8,24},{16,0},{24,8},{1,17},{9,25},{17,1},{25,9},{2,18},{10... | collective-permute-start | bytes 983048 | tf_op jit(solution)/shard_map/ppermute | solution.py:211
  77.8 0.0 collective-permute-done.1.refs_0_
  77.8 0.9 collective-permute-start.12
  78.7 5.1 %collective-permute-done.2.refs_1_ = bf16[160,1024]{1,0:T(8,128)(2,1)S(1)} collective-permute-done((bf16[160,1024]{1,0:T(8,128)(2,1)S(1)}, bf16[160,1024]{1,0:T(8,128)(2,1)S(1)}, u32[]{:S(2)}, u32[]{:S(2)}) %collective-permute-start.2) | collective-permute-done | bytes 327712 | tf_op jit(solution)/shard_map/ppermute | solution.py:211
  83.8 1.4 %collective-permute-done.3.refs_2_ = bf16[160,1024]{1,0:T(8,128)(2,1)S(1)} collective-permute-done((bf16[160,1024]{1,0:T(8,128)(2,1)S(1)}, bf16[160,1024]{1,0:T(8,128)(2,1)S(1)}, u32[]{:S(2)}, u32[]{:S(2)}) %collective-permute-start.3) | collective-permute-done | bytes 327712 | tf_op jit(solution)/shard_map/ppermute | solution.py:211
  85.2 4.2 %expert.4 = (bf16[160,1024]{1,0:T(8,128)(2,1)}, bf16[160,1024]{1,0:T(8,128)(2,1)}, bf16[160,1024]{1,0:T(8,128)(2,1)}) custom-call(bf16[160,1024]{1,0:T(8,128)(2,1)S(1)} %collective-permute-done.1.refs_0_, bf16[160,1024]{1,0:T(8,128)(2,1)S(1)} %collective-permute-done.2.refs_1_, bf16[160,1024]{1,0:T(8,128)(2,1)S(1)} %collective-permute-done.3.refs_2_, ...), custom_call_target="tpu_custom_call" | custom-call | tf_op jit(solution)/shard_map/expert/pallas_call | solution.py:115
  89.3 0.6 collective-permute-start.4
  89.9 1.9 %collective-permute-start.5 = (bf16[160,1024]{1,0:T(8,128)(2,1)}, bf16[160,1024]{1,0:T(8,128)(2,1)}, u32[]{:S(2)}, u32[]{:S(2)}) collective-permute-start(bf16[160,1024]{1,0:T(8,128)(2,1)} %get-tuple-element.16), channel_id=1, source_target_pairs={{0,16},{8,24},{16,0},{24,8},{1,17},{9,25},{17,1},{25,9},{2,18},{10... | collective-permute-start | bytes 983048 | tf_op jit(solution)/shard_map/ppermute | solution.py:211
  91.8 0.0 collective-permute-done.10.refs_4_
  91.9 0.7 copy-done.9
  92.6 1.0 collective-permute-start.6
  93.6 0.1 copy.20
  93.7 0.0 copy-done.15
  93.7 0.8 copy.23.weight_ref
  94.6 1.1 slice_bitcast_fusion.refs_0_
  95.7 0.0 copy-start.2
  95.7 1.6 %copy-done.2 = bf16[1,1024,1024]{2,1,0:T(8,128)(2,1)S(1)} copy-done((bf16[1,1024,1024]{2,1,0:T(8,128)(2,1)S(1)}, bf16[1,1024,1024]{2,1,0:T(8,128)(2,1)}, u32[]{:S(2)}) %copy-start.2) | copy-done | bytes 2097176
  97.3 1.6 %copy-done.4 = bf16[1,1024,1024]{2,1,0:T(8,128)(2,1)S(1)} copy-done((bf16[1,1024,1024]{2,1,0:T(8,128)(2,1)S(1)}, bf16[1,1024,1024]{2,1,0:T(8,128)(2,1)}, u32[]{:S(2)}) %copy-start.4) | copy-done | bytes 2097176
  98.9 2.2 %expert.3.refs_0_ = bf16[320,1024]{1,0:T(8,128)(2,1)S(1)} custom-call(bf16[320,1024]{1,0:T(8,128)(2,1)S(1)} %slice_bitcast_fusion.refs_0_, bf16[1024,1024]{1,0:T(8,128)(2,1)S(1)} %bitcast.40, bf16[1024,1024]{1,0:T(8,128)(2,1)S(1)} %bitcast.43, bf16[1024,1024]{1,0:T(8,128)(2,1)S(1)} %bitcast.46), custom_call_target="tpu_custom_call" | custom-call | tf_op jit(solution)/shard_map/expert/pallas_call | solution.py:115
  101.1 0.0 collective-permute-done.11.refs_5_
  101.1 0.0 collective-permute-done.12.refs_6_
  101.2 2.9 %collective-permute-done.4.refs_1_ = bf16[160,1024]{1,0:T(8,128)(2,1)} collective-permute-done((bf16[160,1024]{1,0:T(8,128)(2,1)}, bf16[160,1024]{1,0:T(8,128)(2,1)}, u32[]{:S(2)}, u32[]{:S(2)}) %collective-permute-start.4) | collective-permute-done | bytes 327712 | tf_op jit(solution)/shard_map/ppermute | solution.py:211
  104.0 6.3 %collective-permute-done.5.refs_2_ = bf16[160,1024]{1,0:T(8,128)(2,1)} collective-permute-done((bf16[160,1024]{1,0:T(8,128)(2,1)}, bf16[160,1024]{1,0:T(8,128)(2,1)}, u32[]{:S(2)}, u32[]{:S(2)}) %collective-permute-start.5) | collective-permute-done | bytes 327712 | tf_op jit(solution)/shard_map/ppermute | solution.py:211
  110.3 1.7 %collective-permute-done.6.refs_3_ = bf16[160,1024]{1,0:T(8,128)(2,1)} collective-permute-done((bf16[160,1024]{1,0:T(8,128)(2,1)}, bf16[160,1024]{1,0:T(8,128)(2,1)}, u32[]{:S(2)}, u32[]{:S(2)}) %collective-permute-start.6) | collective-permute-done | bytes 327712 | tf_op jit(solution)/shard_map/ppermute | solution.py:211
  112.0 0.0 copy-done.5
  112.0 0.0 copy-done.10
  112.0 4.8 %combine.1 = bf16[512,1024]{1,0:T(8,128)(2,1)} custom-call(s32[512,2]{1,0:T(8,128)S(1)} %bitcast.47, f32[512,2]{1,0:T(8,128)S(1)} %copy-done.5, bf16[512,1024]{1,0:T(8,128)(2,1)S(1)} %get-tuple-element.13.mixed_ref, bf16[320,1024]{1,0:T(8,128)(2,1)S(1)} %expert.3.refs_0_, bf16[160,1024]{1,0:T(8,128)(2,1)} %collective-permute-done.4.refs_1_, ...), custom_call_target="tpu_custom_call" | custom-call | tf_op jit(solution)/shard_map/combine/pallas_call | solution.py:146
  (27 shorter events, 0.1 us)
Async XLA Ops:
  0.0 14.3 %copy-start.12 = (bf16[4096,64]{0,1:T(8,128)(2,1)S(1)}, bf16[4096,64]{0,1:T(8,128)(2,1)}, u32[]{:S(2)}) copy-start(bf16[4096,64]{0,1:T(8,128)(2,1)} %param.12) | copy-start | bytes 1572868
  0.0 23.7 %copy-start.13 = (s32[4096]{0:T(1024)S(1)}, s32[4096]{0:T(1024)}, u32[]{:S(2)}) copy-start(s32[4096]{0:T(1024)} %param.15) | copy-start | bytes 49156
  0.0 23.4 %copy-start.14 = (s32[512,2]{0,1:T(2,128)S(1)}, s32[512,2]{0,1:T(2,128)}, u32[]{:S(2)}) copy-start(s32[512,2]{0,1:T(2,128)} %param.22) | copy-start | bytes 12292
  0.0 38.7 %copy-start.11 = (f32[1024]{0:T(1024)S(1)}, f32[1024]{0:T(1024)}, u32[]{:S(2)}) copy-start(f32[1024]{0:T(1024)} %param.18) | copy-start | bytes 12292
  0.0 38.7 %copy-start.6 = (bf16[512,1024]{1,0:T(8,128)(2,1)S(1)}, bf16[512,1024]{1,0:T(8,128)(2,1)}, u32[]{:S(2)}) copy-start(bf16[512,1024]{1,0:T(8,128)(2,1)} %gate_ref.1) | copy-start | bytes 3145732
  2.4 6.2 %collective-permute-start = (bf16[17,64]{1,0:T(8,128)(2,1)S(1)}, bf16[17,64]{1,0:T(8,128)(2,1)S(1)}, u32[]{:S(2)}, u32[]{:S(2)}) collective-permute-start(bf16[17,64]{1,0:T(8,128)(2,1)S(1)} %pad_maximum_fusion.1), channel_id=1, source_target_pairs={{0,8},{8,16},{16,24},{1,9},{9,17},{17,25},{2,10},{10,18},{18,26},{... | collective-permute-start | bytes 6536 | tf_op jit(solution)/shard_map/ppermute | solution.py:183
  9.4 10.5 %all-to-all-start.1 = ((bf16[8,2,512]{2,1,0:T(2,128)(2,1)}), bf16[8,2,512]{2,1,0:T(2,128)(2,1)S(1)}, u32[]{:S(2)}, u32[]{:S(2)}) async-start(bf16[8,2,512]{2,1,0:T(2,128)(2,1)} %reshape.19), calls=%async_computation.1 | async-start | bytes 32768 | tf_op jit(solution)/shard_map/all_to_all | solution.py:189
  19.9 18.8 %all-to-all-start = ((bf16[8,64,512]{2,1,0:T(8,128)(2,1)}), bf16[8,64,512]{2,1,0:T(8,128)(2,1)S(1)}, u32[]{:S(2)}, u32[]{:S(2)}) async-start(bf16[8,64,512]{2,1,0:T(8,128)(2,1)} %bitcast.37), calls=%async_computation | async-start | bytes 1048576 | tf_op jit(solution)/shard_map/all_to_all | solution.py:179
  38.7 1.2 %copy-start.7 = (bf16[512,1024]{1,0:T(8,128)(2,1)S(1)}, bf16[512,1024]{1,0:T(8,128)(2,1)}, u32[]{:S(2)}) copy-start(bf16[512,1024]{1,0:T(8,128)(2,1)} %resid_ref.1) | copy-start | bytes 3145732
  39.9 1.2 %copy-start.8 = (bf16[512,1024]{1,0:T(8,128)(2,1)S(1)}, bf16[512,1024]{1,0:T(8,128)(2,1)}, u32[]{:S(2)}) copy-start(bf16[512,1024]{1,0:T(8,128)(2,1)} %up_ref.1) | copy-start | bytes 3145732
  41.1 30.0 %copy-start.1 = (bf16[1,1024,1024]{2,1,0:T(8,128)(2,1)S(1)}, bf16[1,1024,1024]{2,1,0:T(8,128)(2,1)}, u32[]{:S(2)}) copy-start(bf16[1,1024,1024]{2,1,0:T(8,128)(2,1)} %param.20) | copy-start | bytes 6291460
  41.1 30.0 %copy-start.3 = (bf16[1,1024,1024]{2,1,0:T(8,128)(2,1)S(1)}, bf16[1,1024,1024]{2,1,0:T(8,128)(2,1)}, u32[]{:S(2)}) copy-start(bf16[1,1024,1024]{2,1,0:T(8,128)(2,1)} %param.21) | copy-start | bytes 6291460
  48.9 22.2 %copy-start = (bf16[1,1024,1024]{2,1,0:T(8,128)(2,1)S(1)}, bf16[1,1024,1024]{2,1,0:T(8,128)(2,1)}, u32[]{:S(2)}) copy-start(bf16[1,1024,1024]{2,1,0:T(8,128)(2,1)} %param.19) | copy-start | bytes 6291460
  50.7 10.9 %collective-permute-start.7 = (bf16[160,1024]{1,0:T(8,128)(2,1)S(1)}, bf16[160,1024]{1,0:T(8,128)(2,1)S(1)}, u32[]{:S(2)}, u32[]{:S(2)}) collective-permute-start(bf16[160,1024]{1,0:T(8,128)(2,1)S(1)} %get-tuple-element.23), channel_id=1, source_target_pairs={{0,8},{8,0},{16,24},{24,16},{1,9},{9,1},{17,25},{25,17},{2,10},{10... | collective-permute-start | bytes 983048 | tf_op jit(solution)/shard_map/ppermute | solution.py:211
  53.1 17.2 %collective-permute-start.8 = (bf16[160,1024]{1,0:T(8,128)(2,1)S(1)}, bf16[160,1024]{1,0:T(8,128)(2,1)S(1)}, u32[]{:S(2)}, u32[]{:S(2)}) collective-permute-start(bf16[160,1024]{1,0:T(8,128)(2,1)S(1)} %get-tuple-element.22), channel_id=1, source_target_pairs={{0,16},{8,24},{16,0},{24,8},{1,17},{9,25},{17,1},{25,9},{2,18},{10... | collective-permute-start | bytes 983048 | tf_op jit(solution)/shard_map/ppermute | solution.py:211
  54.6 16.5 %collective-permute-start.9 = (bf16[160,1024]{1,0:T(8,128)(2,1)S(1)}, bf16[160,1024]{1,0:T(8,128)(2,1)S(1)}, u32[]{:S(2)}, u32[]{:S(2)}) collective-permute-start(bf16[160,1024]{1,0:T(8,128)(2,1)S(1)} %get-tuple-element.21), channel_id=1, source_target_pairs={{0,24},{8,16},{16,8},{24,0},{1,25},{9,17},{17,9},{25,1},{2,26},{10... | collective-permute-start | bytes 983048 | tf_op jit(solution)/shard_map/ppermute | solution.py:211
  55.5 22.3 %collective-permute-start.1 = (bf16[160,1024]{1,0:T(8,128)(2,1)S(1)}, bf16[160,1024]{1,0:T(8,128)(2,1)S(1)}, u32[]{:S(2)}, u32[]{:S(2)}) collective-permute-start(bf16[160,1024]{1,0:T(8,128)(2,1)S(1)} %get-tuple-element.26), channel_id=1, source_target_pairs={{0,8},{8,0},{16,24},{24,16},{1,9},{9,1},{17,25},{25,17},{2,10},{10... | collective-permute-start | bytes 983048 | tf_op jit(solution)/shard_map/ppermute | solution.py:211
  56.6 27.2 %collective-permute-start.2 = (bf16[160,1024]{1,0:T(8,128)(2,1)S(1)}, bf16[160,1024]{1,0:T(8,128)(2,1)S(1)}, u32[]{:S(2)}, u32[]{:S(2)}) collective-permute-start(bf16[160,1024]{1,0:T(8,128)(2,1)S(1)} %get-tuple-element.25), channel_id=1, source_target_pairs={{0,16},{8,24},{16,0},{24,8},{1,17},{9,25},{17,1},{25,9},{2,18},{10... | collective-permute-start | bytes 983048 | tf_op jit(solution)/shard_map/ppermute | solution.py:211
  61.6 23.5 %collective-permute-start.3 = (bf16[160,1024]{1,0:T(8,128)(2,1)S(1)}, bf16[160,1024]{1,0:T(8,128)(2,1)S(1)}, u32[]{:S(2)}, u32[]{:S(2)}) collective-permute-start(bf16[160,1024]{1,0:T(8,128)(2,1)S(1)} %get-tuple-element.24), channel_id=1, source_target_pairs={{0,24},{8,16},{16,8},{24,0},{1,25},{9,17},{17,9},{25,1},{2,26},{10... | collective-permute-start | bytes 983048 | tf_op jit(solution)/shard_map/ppermute | solution.py:211
  75.2 16.6 %collective-permute-start.10 = (bf16[160,1024]{1,0:T(8,128)(2,1)S(1)}, bf16[160,1024]{1,0:T(8,128)(2,1)S(1)}, u32[]{:S(2)}, u32[]{:S(2)}) collective-permute-start(bf16[160,1024]{1,0:T(8,128)(2,1)S(1)} %get-tuple-element.18), channel_id=1, source_target_pairs={{0,8},{8,0},{16,24},{24,16},{1,9},{9,1},{17,25},{25,17},{2,10},{10... | collective-permute-start | bytes 983048 | tf_op jit(solution)/shard_map/ppermute | solution.py:211
  75.8 25.3 %collective-permute-start.11 = (bf16[160,1024]{1,0:T(8,128)(2,1)}, bf16[160,1024]{1,0:T(8,128)(2,1)}, u32[]{:S(2)}, u32[]{:S(2)}) collective-permute-start(bf16[160,1024]{1,0:T(8,128)(2,1)} %get-tuple-element.19), channel_id=1, source_target_pairs={{0,16},{8,24},{16,0},{24,8},{1,17},{9,25},{17,1},{25,9},{2,18},{10... | collective-permute-start | bytes 983048 | tf_op jit(solution)/shard_map/ppermute | solution.py:211
  77.8 15.9 %copy-start.15 = (f32[512,2]{0,1:T(2,128)S(1)}, f32[512,2]{0,1:T(2,128)}, u32[]{:S(2)}) copy-start(f32[512,2]{0,1:T(2,128)} %param.23) | copy-start | bytes 12292
  77.8 23.4 %collective-permute-start.12 = (bf16[160,1024]{1,0:T(8,128)(2,1)}, bf16[160,1024]{1,0:T(8,128)(2,1)}, u32[]{:S(2)}, u32[]{:S(2)}) collective-permute-start(bf16[160,1024]{1,0:T(8,128)(2,1)} %get-tuple-element.20), channel_id=1, source_target_pairs={{0,24},{8,16},{16,8},{24,0},{1,25},{9,17},{17,9},{25,1},{2,26},{10... | collective-permute-start | bytes 983048 | tf_op jit(solution)/shard_map/ppermute | solution.py:211
  89.3 14.7 %collective-permute-start.4 = (bf16[160,1024]{1,0:T(8,128)(2,1)}, bf16[160,1024]{1,0:T(8,128)(2,1)}, u32[]{:S(2)}, u32[]{:S(2)}) collective-permute-start(bf16[160,1024]{1,0:T(8,128)(2,1)} %get-tuple-element.15), channel_id=1, source_target_pairs={{0,8},{8,0},{16,24},{24,16},{1,9},{9,1},{17,25},{25,17},{2,10},{10... | collective-permute-start | bytes 983048 | tf_op jit(solution)/shard_map/ppermute | solution.py:211
  89.9 20.3 %collective-permute-start.5 = (bf16[160,1024]{1,0:T(8,128)(2,1)}, bf16[160,1024]{1,0:T(8,128)(2,1)}, u32[]{:S(2)}, u32[]{:S(2)}) collective-permute-start(bf16[160,1024]{1,0:T(8,128)(2,1)} %get-tuple-element.16), channel_id=1, source_target_pairs={{0,16},{8,24},{16,0},{24,8},{1,17},{9,25},{17,1},{25,9},{2,18},{10... | collective-permute-start | bytes 983048 | tf_op jit(solution)/shard_map/ppermute | solution.py:211
  91.9 0.7 copy-start.9
  92.6 19.4 %collective-permute-start.6 = (bf16[160,1024]{1,0:T(8,128)(2,1)}, bf16[160,1024]{1,0:T(8,128)(2,1)}, u32[]{:S(2)}, u32[]{:S(2)}) collective-permute-start(bf16[160,1024]{1,0:T(8,128)(2,1)} %get-tuple-element.17), channel_id=1, source_target_pairs={{0,24},{8,16},{16,8},{24,0},{1,25},{9,17},{17,9},{25,1},{2,26},{10... | collective-permute-start | bytes 983048 | tf_op jit(solution)/shard_map/ppermute | solution.py:211
  95.7 1.6 %copy-start.2 = (bf16[1,1024,1024]{2,1,0:T(8,128)(2,1)S(1)}, bf16[1,1024,1024]{2,1,0:T(8,128)(2,1)}, u32[]{:S(2)}) copy-start(bf16[1,1024,1024]{2,1,0:T(8,128)(2,1)} %param.20) | copy-start | bytes 6291460
  97.3 1.6 %copy-start.4 = (bf16[1,1024,1024]{2,1,0:T(8,128)(2,1)S(1)}, bf16[1,1024,1024]{2,1,0:T(8,128)(2,1)}, u32[]{:S(2)}) copy-start(bf16[1,1024,1024]{2,1,0:T(8,128)(2,1)} %param.21) | copy-start | bytes 6291460
  98.9 13.1 %copy-start.5 = (f32[512,2]{1,0:T(8,128)S(1)}, f32[512,2]{1,0:T(8,128)}, u32[]{:S(2)}) copy-start(f32[512,2]{1,0:T(8,128)} %copy.23.weight_ref) | copy-start | bytes 12292
  98.9 13.1 %copy-start.10 = (bf16[160,1024]{1,0:T(8,128)(2,1)S(1)}, bf16[160,1024]{1,0:T(8,128)(2,1)}, u32[]{:S(2)}) copy-start(bf16[160,1024]{1,0:T(8,128)(2,1)} %copy-done.9) | copy-start | bytes 983044
